TPU v7x, 32 devices: a whole 2x2x4 slice. The times are simulated.
32 devices in a mesh: rep: 2 (over y), fs: 4 (over z), tp: 4 (over x, core).
Axes of the slice: x: 2, y: 2, z: 4, core: 2. Of those that a mesh axis runs over, the one named last changes fastest.
Arguments:
- gate_pre: bfloat16 [8192, 3072], P(('rep', 'fs'), 'tp'), may hold values from -6 to 6
- up_pre: bfloat16 [8192, 3072], P(('rep', 'fs'), 'tp'), may hold values from -6 to 6
- out_grad: bfloat16 [8192, 2048], P(('rep', 'fs')), may hold values from -8 to 8
- w_down: bfloat16 [3072, 2048], P('tp', 'fs'), may hold values from -0.109375 to 0.109375
Outputs:
- d_gate: bfloat16 [8192, 3072], P(('rep', 'fs'), 'tp')
- d_up: bfloat16 [8192, 3072], P(('rep', 'fs'), 'tp')
- grad_down: float32 [3072, 2048], P('tp', 'fs')
- row_energy: float32 [3072], P('tp')
All inputs are finite; a program needn't handle non-finite values.
Results may differ from a plain program's by a relative error of at most 0.0034.
Values may be sent and summed in bfloat16 or wider, within the bound.
A program may use at most 64 MiB of HBM per device.

v0:
```python
import jax
import jax.numpy as jnp
from jax import lax
from jax.sharding import PartitionSpec as P

D = 2048


def local(gate_pre, up_pre, out_grad, w_down):
    gate_f = gate_pre.astype(jnp.float32)
    up_f = up_pre.astype(jnp.float32)
    sig = jax.nn.sigmoid(gate_f)
    act = gate_f * sig
    hidden = (act * up_f).astype(jnp.bfloat16)
    tokens_all = out_grad.shape[0] * lax.axis_size("rep") * lax.axis_size("fs")
    factor = float(tokens_all) ** (-0.5)
    weight_whole = lax.all_gather(w_down, "fs", axis=1, tiled=True)
    dhid = lax.dot_general(
        out_grad, weight_whole, (((1,), (1,)), ((), ())), preferred_element_type=jnp.float32
    )
    d_up = (dhid * act).astype(jnp.bfloat16)
    d_gate = (dhid * up_f * sig * (1.0 + gate_f * (1.0 - sig))).astype(jnp.bfloat16)
    d_gate, d_up = (d_gate, d_up)
    shard = lax.psum_scatter(
        lax.dot_general(
            out_grad, hidden, (((0,), (0,)), ((), ())), preferred_element_type=jnp.float32
        ),
        "fs",
        scatter_dimension=0,
        tiled=True,
    )
    shard = lax.psum(shard, "rep")
    grad_down = shard.T * factor
    energy = lax.psum(jnp.sum(grad_down * grad_down, axis=1), "fs") / D
    return (d_gate, d_up, grad_down, energy)


def solution(mesh):
    placed = (P(("rep", "fs"), "tp"), P(("rep", "fs"), "tp"), P(("rep", "fs"), None), P("tp", "fs"))
    return jax.shard_map(
        local,
        mesh=mesh,
        in_specs=placed,
        out_specs=(P(("rep", "fs"), "tp"), P(("rep", "fs"), "tp"), P("tp", "fs"), P("tp")),
        check_vma=False,
    )
```

profile of v0, /device:TPU:0, one launch (start us, length us, event | category | flops | bytes accessed | tf_op | source)
XLA Modules:
  0.0 269.9 jit_solution(15199787096322260005)
XLA Ops:
  7.2 0.0 reduce-scatter.2.cloned.1.call-start
  7.2 9.4 %convolution_bitcast_fusion = f32[2048,768]{0,1:T(8,128)} fusion(bf16[1024,2048]{1,0:T(8,128)(2,1)} %param.6, bf16[1024,768]{1,0:T(8,128)(2,1)} %param.5, bf16[1024,768]{1,0:T(8,128)(2,1)} %param.4), kind=kOutput, calls=%fused_computation.5 | convolution fusion | flops 3227516928 | bytes 13631488 | tf_op jit(solution)/shard_map/dot_general | solution.py:25
  16.6 0.0 copy-start
  16.7 0.0 copy-start.1
  16.7 0.0 reduce-scatter.2.cloned.1.call-update
  16.7 0.0 all-gather.2.cloned.1.call-start
  16.7 0.7 all-gather.2.cloned.1.call-update
  17.4 0.0 all-reduce.2.cloned.1.call-start
  17.5 112.9 %reduce-scatter.2.cloned.1.call-done = f32[512,768]{0,1:T(8,128)} async-done(((f32[2048,768]{0,1:T(8,128)}), f32[512,768]{0,1:T(8,128)}) %reduce-scatter.2.cloned.1.call-update) | async-done | bytes 1572880 | tf_op jit(solution)/shard_map/reduce_scatter | solution.py:24
  130.4 0.0 all-reduce.2.cloned.1.call-update
  130.4 65.5 %all-gather.2.cloned.1.call-done = bf16[768,2048]{1,0:T(8,128)(2,1)} async-done(((bf16[768,512]{1,0:T(8,128)(2,1)}), bf16[768,2048]{1,0:T(8,128)(2,1)}) %all-gather.2.cloned.1.call-update) | async-done | bytes 3145744 | tf_op jit(solution)/shard_map/all_gather | solution.py:17
  195.9 0.0 copy-done
  195.9 0.0 copy-done.1
  195.9 9.2 %multiply_convert_fusion = (bf16[1024,768]{1,0:T(8,128)(2,1)}, bf16[1024,768]{1,0:T(8,128)(2,1)}) fusion(bf16[1024,768]{1,0:T(8,128)(2,1)S(1)} %copy-done, bf16[1024,768]{1,0:T(8,128)(2,1)S(1)} %copy-done.1, bf16[1024,2048]{1,0:T(8,128)(2,1)} %param.6, bf16[768,2048]{1,0:T(8,128)(2,1)} %all-gather.2.cloned.1.call-done), kind=kOutput, calls=%fused_computation.14 | convolution fusion | flops 3233021952 | bytes 13631488 | tf_op jit(solution)/shard_map/dot_general | solution.py:18
  205.0 43.4 %all-reduce.2.cloned.1.call-done = f32[512,768]{0,1:T(8,128)} async-done(((f32[512,768]{0,1:T(8,128)}), f32[512,768]{0,1:T(8,128)}) %all-reduce.2.cloned.1.call-update) | async-done | bytes 1572880 | tf_op jit(solution)/shard_map/psum | solution.py:32
  248.4 2.7 multiply_reduce_fusion
  251.1 11.7 %psum.15 = f32[768]{0:T(1024)S(1)} all-reduce(f32[768]{0:T(1024)S(1)} %get-tuple-element.4), channel_id=1, replica_groups=mesh['rep'=2,'fs'=4,'tp'=4] {'fs'}, use_global_device_ids=true, to_apply=%region_3.0 | all-reduce | flops 768 | bytes 6144 | tf_op jit(solution)/shard_map/psum | solution.py:34
  262.8 0.6 broadcast_multiply_fusion
Async XLA Ops:
  7.2 123.2 %reduce-scatter.2.cloned.1.call-start = ((), (), s32[]{:S(2)}) async-start(), calls=%async_computation.2 | async-start | bytes 7864320 | tf_op jit(solution)/shard_map/reduce_scatter | solution.py:24
  16.6 179.2 %copy-start = (bf16[1024,768]{1,0:T(8,128)(2,1)S(1)}, bf16[1024,768]{1,0:T(8,128)(2,1)}, u32[]{:S(2)}) copy-start(bf16[1024,768]{1,0:T(8,128)(2,1)} %param.4) | copy-start | bytes 4718596
  16.7 179.2 %copy-start.1 = (bf16[1024,768]{1,0:T(8,128)(2,1)S(1)}, bf16[1024,768]{1,0:T(8,128)(2,1)}, u32[]{:S(2)}) copy-start(bf16[1024,768]{1,0:T(8,128)(2,1)} %param.5) | copy-start | bytes 4718596
  16.7 179.2 %all-gather.2.cloned.1.call-start = ((), (), s32[]{:S(2)}) async-start(), calls=%async_computation.1 | async-start | bytes 3932160 | tf_op jit(solution)/shard_map/all_gather | solution.py:17
  17.4 231.0 %all-reduce.2.cloned.1.call-start = ((), (), s32[]{:S(2)}) async-start(), calls=%async_computation.3 | async-start | bytes 3145728 | tf_op jit(solution)/shard_map/psum | solution.py:32
Sparse Core Ops, SparseCore 0:
  16.8 113.5 reduce-scatter.1
  131.9 63.9 all-gather.1
  198.2 50.1 all-reduce.1
where the time goes:
time: 270 us
  waiting for transfers between devices  222 us (82%)
  matrix products  18.6 us (7%)
  between operations  13.7 us (5%)
  blocking collectives  11.7 us (4%)
  other arithmetic  3.29 us (1%)
    reduce_scatter x1, waiting for transfers between devices, local(): lax.psum_scatter(lax.dot_general(out_grad, hidden, (((0,), (0,)), ((), ()...  113 us
    all_gather x1, waiting for transfers between devices, local(): weight_whole = lax.all_gather(w_down, 'fs', axis=1, tiled=True)  65.5 us
    psum x1, waiting for transfers between devices, local(): shard = lax.psum(shard, 'rep')  43.4 us
    psum x1, blocking collectives, local(): energy = lax.psum(jnp.sum(grad_down * grad_down, axis=1), 'fs') / D  11.7 us
    dot_general x1, matrix products, local(): lax.dot_general(out_grad, hidden, (((0,), (0,)), ((), ())), preferred_ele...  9.44 us
    dot_general x1, matrix products, local(): lax.dot_general(out_grad, weight_whole, (((1,), (1,)), ((), ())), preferr...  9.15 us
  transfers between devices with their start and end apart: 3, of which 3 were waited for; matrix products, arithmetic and copies ran while one was open for 3% of the time, Pallas kernels for 0%

commit v1 on v0

v1 whole, which is shorter than its diff:
```python
import functools

import jax
import jax.numpy as jnp
from jax import lax
from jax.experimental import pallas as pl
from jax.experimental.pallas import tpu as pltpu
from jax.sharding import PartitionSpec as P

MESH = pl.DeviceIdType.MESH
F32 = jnp.float32
BF16 = jnp.bfloat16
PIECES = 8
SPLIT = 2
LAG = 2


def plain(gate_pre, up_pre, out_grad, w_down):
    gate_f = gate_pre.astype(F32)
    up_f = up_pre.astype(F32)
    sig = jax.nn.sigmoid(gate_f)
    act = gate_f * sig
    hidden = (act * up_f).astype(BF16)
    tokens_all = out_grad.shape[0] * lax.axis_size("rep") * lax.axis_size("fs")
    factor = float(tokens_all) ** (-0.5)
    weight_whole = lax.all_gather(w_down, "fs", axis=1, tiled=True)
    dhid = lax.dot_general(out_grad, weight_whole, (((1,), (1,)), ((), ())), preferred_element_type=F32)
    d_up = (dhid * act).astype(BF16)
    d_gate = (dhid * up_f * sig * (1.0 + gate_f * (1.0 - sig))).astype(BF16)
    shard = lax.psum_scatter(
        lax.dot_general(out_grad, hidden, (((0,), (0,)), ((), ())), preferred_element_type=F32),
        "fs",
        scatter_dimension=0,
        tiled=True,
    )
    shard = lax.psum(shard, "rep")
    grad_down = shard.T * factor
    energy = lax.psum(jnp.sum(grad_down * grad_down, axis=1), "fs") / out_grad.shape[1]
    return (d_gate, d_up, grad_down, energy)


def kernel(
    n, factor, width,
    g_hbm, u_hbm, og_hbm, w_hbm,
    dg_hbm, du_hbm, gd_hbm, en_ref,
    g, u, og, dg, du, gd, w, hid, part, zsend, zrecv, ysend, yrecv, fsend, frecv, lanes, esend, erecv,
    in_sem, out_sem, gd_sem, zs_sem, zr_sem, as_sem, ar_sem, ys_sem, yr_sem, fs_sem, fr_sem, es_sem, er_sem,
):
    rep = lax.axis_index("rep")
    k = lax.axis_index("fs")
    mate = 1 - rep
    cols = w.shape[3]
    hidden_units = g.shape[1]
    tokens = g.shape[0]
    count = PIECES - SPLIT

    def piece(c):
        return c + jnp.where(c < SPLIT, rep * SPLIT, SPLIT)

    def loop(lo, hi, body):
        lax.fori_loop(lo, hi, lambda i, x: (body(i), x)[1], 0)

    in_w = pltpu.make_async_copy(w_hbm, w.at[k], in_sem.at[0])
    in_g = pltpu.make_async_copy(g_hbm, g, in_sem.at[1])
    in_u = pltpu.make_async_copy(u_hbm, u, in_sem.at[2])
    in_og = [
        pltpu.make_async_copy(og_hbm.at[:, pl.ds(j * cols, cols)], og.at[j], in_sem.at[3 + j]) for j in range(n)
    ]
    in_w.start()
    in_g.start()
    in_u.start()
    for j in range(n):
        in_og[j].start()

    barrier = pltpu.get_barrier_semaphore()
    for t in range(1, n):
        pl.semaphore_signal(barrier, inc=1, device_id={"fs": lax.rem(k + t, n)}, device_id_type=MESH)
    pl.semaphore_signal(barrier, inc=1, device_id={"rep": mate}, device_id_type=MESH)
    pl.semaphore_wait(barrier, n)
    in_w.wait()

    at = (k, n - 1 - k)
    sign = (1, -1)

    def along(d, s, c, src, dst):
        return pltpu.make_async_remote_copy(
            src_ref=src, dst_ref=dst, send_sem=zs_sem.at[d, s, c], recv_sem=zr_sem.at[d, s, c],
            device_id={"fs": k + sign[d]}, device_id_type=MESH,
        )

    def across(src, dst, send, recv):
        return pltpu.make_async_remote_copy(
            src_ref=src, dst_ref=dst, send_sem=send, recv_sem=recv,
            device_id={"rep": mate}, device_id_type=MESH,
        )

    def first(c):
        for d in range(2):

            @pl.when(at[d] < n - 1)
            def _():
                block = w.at[k, piece(c)]
                along(d, 0, c, block, block).start()

    loop(0, count, first)

    in_g.wait()
    in_u.wait()
    rows = tokens // 8

    def make_hidden(i):
        at_rows = pl.ds(pl.multiple_of(i * rows, rows), rows)
        gate = g[at_rows, :].astype(F32)
        act = gate * jax.nn.sigmoid(gate)
        h = (act * u[at_rows, :].astype(F32)).astype(BF16)
        hid[:, at_rows] = h.T

    loop(0, 8, make_hidden)
    for j in range(n):
        in_og[j].wait()

    def make_part(i):
        j = jnp.where(i % 2 == 0, n - 1 - i // 2, i // 2)
        part[j] = jnp.dot(hid[...], og[j], preferred_element_type=F32).reshape(part.shape[1:])
        ysend[j] = part[j, pl.ds(mate * SPLIT, SPLIT)].astype(BF16)
        across(ysend.at[j], yrecv.at[j], ys_sem.at[j], yr_sem.at[j]).start()

    loop(0, n, make_part)

    def pass_on(s, c):
        p = piece(c)
        for d in range(2):
            place = at[d]

            @pl.when(place > 0)
            def _():
                along(d, s - 1, c, zsend.at[d, 0, c], zrecv.at[d, 0, c]).wait_recv()

            @pl.when(s <= place)
            def _():
                block = w.at[k - sign[d] * s, p]

                @pl.when(place < n - 1)
                def _():
                    along(d, s, c, block, block).start()

                @pl.when(c < SPLIT)
                def _():
                    j = k - sign[d] * s
                    across(block, block, as_sem.at[j, c], ar_sem.at[j, c]).start()

            @pl.when(s > place)
            def _():
                j = k + sign[d] * (n - s)

                @pl.when(c == 0)
                def _():
                    across(ysend.at[j], yrecv.at[j], ys_sem.at[j], yr_sem.at[j]).wait_recv()

                @pl.when(c < SPLIT)
                def _():
                    part[j, p] += yrecv[j, jnp.minimum(c, SPLIT - 1)].astype(F32)

                if s > 1:

                    @pl.when(place > 0)
                    def _():
                        part[j, p] += zrecv[d, s - 2, c].astype(F32)

                zsend[d, s - 1, c] = part[j, p].astype(BF16)
                along(d, s, c, zsend.at[d, s - 1, c], zrecv.at[d, s - 1, c]).start()

    for s in range(1, n):
        loop(0, count, functools.partial(pass_on, s))

    def finish(c):
        p = piece(c)

        @pl.when(c == 0)
        def _():
            across(ysend.at[k], yrecv.at[k], ys_sem.at[k], yr_sem.at[k]).wait_recv()

        @pl.when(c < SPLIT)
        def _():
            part[k, p] += yrecv[k, jnp.minimum(c, SPLIT - 1)].astype(F32)

        for d in range(2):

            @pl.when(at[d] > 0)
            def _():
                along(d, n - 1, c, zsend.at[d, n - 2, c], zrecv.at[d, n - 2, c]).wait_recv()
                part[k, p] += zrecv[d, n - 2, c].astype(F32)

        fsend[c] = part[k, p].astype(BF16)
        across(fsend.at[c], frecv.at[c], fs_sem.at[c], fr_sem.at[c]).start()

    def put(p, value):
        gd[p] = value
        sq = value * value
        total = sq[:, :128]
        for b in range(1, cols // 128):
            total += sq[:, b * 128 : (b + 1) * 128]
        lanes[p] = total
        pltpu.make_async_copy(gd.at[p], gd_hbm.at[p], gd_sem.at[p]).start()

    def deliver(c):
        across(fsend.at[c], frecv.at[c], fs_sem.at[c], fr_sem.at[c]).wait_recv()

        @pl.when(c < SPLIT)
        def _():
            put(rep * SPLIT + c, fsend[c].astype(F32) * factor)
            put(mate * SPLIT + c, frecv[c].astype(F32) * factor)

        @pl.when(c >= SPLIT)
        def _():
            put(c + SPLIT, (fsend[c].astype(F32) + frecv[c].astype(F32)) * factor)

    blocks = 4
    brows = tokens // blocks

    def activations(i):
        at_rows = pl.ds(pl.multiple_of(i * brows, brows), brows)
        dhid = jnp.zeros((brows, hidden_units), F32)
        for j in range(n):
            dhid += lax.dot_general(
                og[j, at_rows, :], w[j].reshape(hidden_units, cols), (((1,), (1,)), ((), ())),
                preferred_element_type=F32,
            )
        gate = g[at_rows, :].astype(F32)
        up = u[at_rows, :].astype(F32)
        sig = jax.nn.sigmoid(gate)
        du[at_rows, :] = (dhid * (gate * sig)).astype(BF16)
        dg[at_rows, :] = (dhid * up * sig * (1.0 + gate * (1.0 - sig))).astype(BF16)
        pltpu.make_async_copy(du.at[at_rows], du_hbm.at[at_rows], out_sem.at[0, i]).start()
        pltpu.make_async_copy(dg.at[at_rows], dg_hbm.at[at_rows], out_sem.at[1, i]).start()

    def gathered(j):
        @pl.when(j != k)
        def _():
            for c in range(SPLIT):
                block = w.at[j, mate * SPLIT + c]
                across(block, block, as_sem.at[j, c], ar_sem.at[j, c]).wait_recv()

    def last(c):
        @pl.when(c < count)
        def _():
            finish(c)

        @pl.when(c == 0)
        def _():
            loop(0, n, gathered)

        @pl.when(c < blocks)
        def _():
            activations(c)

        @pl.when(c >= LAG)
        def _():
            deliver(c - LAG)

    loop(0, count + LAG, last)

    row = jnp.sum(lanes[...].reshape(hidden_units, 128).T, axis=0, keepdims=True)
    esend[...] = jnp.broadcast_to(row, esend.shape)

    def energy_copy(to, slot):
        return pltpu.make_async_remote_copy(
            src_ref=esend, dst_ref=erecv.at[slot], send_sem=es_sem.at[to], recv_sem=er_sem.at[slot],
            device_id={"fs": to}, device_id_type=MESH,
        )

    for t in range(1, n):
        energy_copy(lax.rem(k + t, n), k).start()

    def sent(c):
        for d in range(2):

            @pl.when(at[d] < n - 1)
            def _():
                for s in range(n):
                    along(d, s, c, zsend.at[d, 0, c], zrecv.at[d, 0, c]).wait_send()

        across(fsend.at[c], frecv.at[c], fs_sem.at[c], fr_sem.at[c]).wait_send()

    loop(0, count, sent)

    def sent_across(j):
        across(ysend.at[j], yrecv.at[j], ys_sem.at[j], yr_sem.at[j]).wait_send()

        @pl.when(j != k)
        def _():
            for c in range(SPLIT):
                block = w.at[j, rep * SPLIT + c]
                across(block, block, as_sem.at[j, c], ar_sem.at[j, c]).wait_send()

    loop(0, n, sent_across)

    def stored(i):
        at_rows = pl.ds(pl.multiple_of(i * brows, brows), brows)
        pltpu.make_async_copy(du.at[at_rows], du_hbm.at[at_rows], out_sem.at[0, i]).wait()
        pltpu.make_async_copy(dg.at[at_rows], dg_hbm.at[at_rows], out_sem.at[1, i]).wait()

    loop(0, blocks, stored)
    loop(0, PIECES, lambda p: pltpu.make_async_copy(gd.at[p], gd_hbm.at[p], gd_sem.at[p]).wait())

    for t in range(1, n):
        energy_copy(k, lax.rem(k + t, n)).wait_recv()
    total = jnp.zeros((8, hidden_units), F32)
    for j in range(n):
        total += jnp.where(j == k, esend[...], erecv[j])
    en_ref[...] = total[:1] * (1.0 / width)
    for t in range(1, n):
        energy_copy(lax.rem(k + t, n), k).wait_send()


def fused(n, gate_pre, up_pre, out_grad, w_down):
    tokens, units = gate_pre.shape
    width = out_grad.shape[1]
    cols = w_down.shape[1]
    rows = units // PIECES
    count = PIECES - SPLIT
    factor = float(tokens * lax.axis_size("rep") * n) ** (-0.5)
    any_spec = pl.BlockSpec(memory_space=pl.ANY)
    dma = pltpu.SemaphoreType.DMA
    d_gate, d_up, grad, energy = pl.pallas_call(
        functools.partial(kernel, n, factor, width),
        out_shape=(
            jax.ShapeDtypeStruct((tokens, units), BF16),
            jax.ShapeDtypeStruct((tokens, units), BF16),
            jax.ShapeDtypeStruct((PIECES, rows, cols), F32),
            jax.ShapeDtypeStruct((1, units), F32),
        ),
        in_specs=[any_spec] * 4,
        out_specs=(any_spec, any_spec, any_spec, pl.BlockSpec(memory_space=pltpu.VMEM)),
        scratch_shapes=[
            pltpu.VMEM((tokens, units), BF16),
            pltpu.VMEM((tokens, units), BF16),
            pltpu.VMEM((n, tokens, cols), BF16),
            pltpu.VMEM((tokens, units), BF16),
            pltpu.VMEM((tokens, units), BF16),
            pltpu.VMEM((PIECES, rows, cols), F32),
            pltpu.VMEM((n, PIECES, rows, cols), BF16),
            pltpu.VMEM((units, tokens), BF16),
            pltpu.VMEM((n, PIECES, rows, cols), F32),
            pltpu.VMEM((2, n - 1, count, rows, cols), BF16),
            pltpu.VMEM((2, n - 1, count, rows, cols), BF16),
            pltpu.VMEM((n, SPLIT, rows, cols), BF16),
            pltpu.VMEM((n, SPLIT, rows, cols), BF16),
            pltpu.VMEM((count, rows, cols), BF16),
            pltpu.VMEM((count, rows, cols), BF16),
            pltpu.VMEM((PIECES, rows, 128), F32),
            pltpu.VMEM((8, units), F32),
            pltpu.VMEM((n, 8, units), F32),
            dma((3 + n,)),
            dma((2, 4)),
            dma((PIECES,)),
            dma((2, n, count)),
            dma((2, n, count)),
            dma((n, SPLIT)),
            dma((n, SPLIT)),
            dma((n,)),
            dma((n,)),
            dma((count,)),
            dma((count,)),
            dma((n,)),
            dma((n,)),
        ],
        compiler_params=pltpu.CompilerParams(
            collective_id=0, has_side_effects=True, vmem_limit_bytes=60 * 1024 * 1024
        ),
    )(gate_pre, up_pre, out_grad, w_down.reshape(PIECES, rows, cols))
    return d_gate, d_up, grad.reshape(units, cols), energy.reshape(units)


def solution(mesh):
    reps, n = mesh.shape["rep"], mesh.shape["fs"]

    def local(gate_pre, up_pre, out_grad, w_down):
        units, cols = w_down.shape
        fits = reps == 2 and 2 <= n <= 4 and cols % 128 == 0 and units % (PIECES * 16) == 0 and units % 128 == 0
        if fits and gate_pre.shape[0] % 1024 == 0:
            return fused(n, gate_pre, up_pre, out_grad, w_down)
        return plain(gate_pre, up_pre, out_grad, w_down)

    placed = (P(("rep", "fs"), "tp"), P(("rep", "fs"), "tp"), P(("rep", "fs"), None), P("tp", "fs"))
    return jax.shard_map(
        local,
        mesh=mesh,
        in_specs=placed,
        out_specs=(P(("rep", "fs"), "tp"), P(("rep", "fs"), "tp"), P("tp", "fs"), P("tp")),
        check_vma=False,
    )
```

time: 270 us -> 75.3 us (0.28)
  waiting for transfers between devices: 222 us -> 0 us
  Pallas kernels: 0 us -> 67.3 us
  matrix products: 18.6 us -> 0 us
  between operations: 13.7 us -> 0.64 us
  blocking collectives: 11.7 us -> 0 us
  local copies, waits for them, and re-layouts: 0.01 us -> 5.89 us
    reduce_scatter x1 -> x0, waiting for transfers between devices: 113 us -> none  [local(): lax.psum_scatter(lax.dot_general(out_grad, hidden, (((0,), (0,)), ((), ()...]
    pallas_call x0 -> x1, Pallas kernels: none -> 67.3 us  [fused(): pl.pallas_call(functools.partial(kernel, n, factor, width), out_shape=(ja...]
    all_gather x1 -> x0, waiting for transfers between devices: 65.5 us -> none  [local(): weight_whole = lax.all_gather(w_down, 'fs', axis=1, tiled=True)]
    psum x1 -> x0, waiting for transfers between devices: 43.4 us -> none  [local(): shard = lax.psum(shard, 'rep')]
    dot_general x2 -> x0, matrix products: 18.6 us -> none  [the longest x1 9.44 us: local(): lax.dot_general(out_grad, hidden, (((0,), (0,)), ((), ())), preferred_ele...]
    psum x1 -> x0, blocking collectives: 11.7 us -> none  [local(): energy = lax.psum(jnp.sum(grad_down * grad_down, axis=1), 'fs') / D]
    unnamed x4 -> x7, local copies, waits for them, and re-layouts: 0.01 us -> 5.89 us
  transfers between devices with their start and end apart: 3 -> 0, of which waited for: 3 -> 0; matrix products, arithmetic and copies ran while one was open for 3% -> 0% of each run, Pallas kernels for 0% -> 0%
where the time goes in v1:
time: 75.3 us; the launch traced here: 75.1 us
  Pallas kernels  67.3 us (89%)
  local copies, waits for them, and re-layouts  5.89 us (8%)
  other arithmetic  1.28 us (2%)
    pallas_call x1, Pallas kernels, fused(): pl.pallas_call(functools.partial(kernel, n, factor, width), out_shape=(ja...  67.3 us
    unnamed x7, local copies, waits for them, and re-layouts  5.89 us

profile of v1, /device:TPU:0, one launch (start us, length us, event | category | flops | bytes accessed | tf_op | source)
XLA Modules:
  0.0 75.1 jit_solution(7654739351468670852)
XLA Ops:
  0.6 67.3 %shard_map.75 = (bf16[1024,768]{1,0:T(8,128)(2,1)}, bf16[1024,768]{1,0:T(8,128)(2,1)}, f32[8,96,512]{2,1,0:T(8,128)}, f32[1,768]{1,0:T(1,128)}) custom-call(bf16[1024,768]{1,0:T(8,128)(2,1)} %g_hbm.1, bf16[1024,768]{1,0:T(8,128)(2,1)} %u_hbm.1, bf16[1024,2048]{1,0:T(8,128)(2,1)} %og_hbm.1, bf16[8,96,512]{2,1,0:T(8,128)(2,1)} %bitcast.3), custom_call_target="tpu_custom_call" | custom-call | tf_op jit(solution)/shard_map/pallas_call | solution.py:325
  67.9 1.3 %reduce = f32[768]{0:T(1024)} reduce(f32[1,768]{1,0:T(1,128)} %get-tuple-element.11, f32[]{:T(128)} %constant), dimensions={0}, to_apply=%get-tuple-element.11.reduce_sub_computation | reduce | bytes 6148 | tf_op jit(solution)/shard_map/pallas_call | solution.py:325
  69.2 0.0 copy-start.1
  69.2 2.8 %copy.11 = bf16[1024,768]{1,0:T(8,128)(2,1)} copy(bf16[1024,768]{1,0:T(8,128)(2,1)} %get-tuple-element.16) | data formatting | bytes 3145728
  72.0 0.0 copy-done.1
  72.0 0.0 copy-start
  72.0 1.1 %copy.12 = bf16[1024,768]{1,0:T(8,128)(2,1)} copy(bf16[1024,768]{1,0:T(8,128)(2,1)S(1)} %copy-done.1) | data formatting | bytes 3145728
  73.1 0.8 %copy-done = f32[8,96,512]{2,1,0:T(8,128)S(1)} copy-done((f32[8,96,512]{2,1,0:T(8,128)S(1)}, f32[8,96,512]{2,1,0:T(8,128)}, u32[]{:S(2)}) %copy-start) | copy-done | bytes 1572888
  74.0 1.1 %copy.13 = f32[768,512]{1,0:T(8,128)} copy(f32[768,512]{1,0:T(8,128)S(1)} %bitcast.2) | data formatting | bytes 3145728
Async XLA Ops:
  69.2 2.8 %copy-start.1 = (bf16[1024,768]{1,0:T(8,128)(2,1)S(1)}, bf16[1024,768]{1,0:T(8,128)(2,1)}, u32[]{:S(2)}) copy-start(bf16[1024,768]{1,0:T(8,128)(2,1)} %get-tuple-element.17) | copy-start | bytes 4718596
  72.0 2.0 %copy-start = (f32[8,96,512]{2,1,0:T(8,128)S(1)}, f32[8,96,512]{2,1,0:T(8,128)}, u32[]{:S(2)}) copy-start(f32[8,96,512]{2,1,0:T(8,128)} %get-tuple-element.10) | copy-start | bytes 4718596

commit v2 on v1

--- a/solution.py
+++ b/solution.py
@@ -10,9 +10,10 @@
 MESH = pl.DeviceIdType.MESH
 F32 = jnp.float32
 BF16 = jnp.bfloat16
-PIECES = 8
+PIECES = 6
 SPLIT = 2
 LAG = 2
+VMEM_LIMIT = 52 * 1024 * 1024
 
 
 def plain(gate_pre, up_pre, out_grad, w_down):
@@ -42,9 +43,9 @@
 def kernel(
     n, factor, width,
     g_hbm, u_hbm, og_hbm, w_hbm,
-    dg_hbm, du_hbm, gd_hbm, en_ref,
-    g, u, og, dg, du, gd, w, hid, part, zsend, zrecv, ysend, yrecv, fsend, frecv, lanes, esend, erecv,
-    in_sem, out_sem, gd_sem, zs_sem, zr_sem, as_sem, ar_sem, ys_sem, yr_sem, fs_sem, fr_sem, es_sem, er_sem,
+    dg, du, gd, en_ref,
+    g, u, og, w, hid, part, zsend, zrecv, ysend, yrecv, fsend, frecv, lanes, esend, erecv,
+    in_sem, zs_sem, zr_sem, as_sem, ar_sem, ys_sem, yr_sem, fs_sem, fr_sem, es_sem, er_sem,
 ):
     rep = lax.axis_index("rep")
     k = lax.axis_index("fs")
@@ -201,7 +202,6 @@
         for b in range(1, cols // 128):
             total += sq[:, b * 128 : (b + 1) * 128]
         lanes[p] = total
-        pltpu.make_async_copy(gd.at[p], gd_hbm.at[p], gd_sem.at[p]).start()
 
     def deliver(c):
         across(fsend.at[c], frecv.at[c], fs_sem.at[c], fr_sem.at[c]).wait_recv()
@@ -231,8 +231,6 @@
         sig = jax.nn.sigmoid(gate)
         du[at_rows, :] = (dhid * (gate * sig)).astype(BF16)
         dg[at_rows, :] = (dhid * up * sig * (1.0 + gate * (1.0 - sig))).astype(BF16)
-        pltpu.make_async_copy(du.at[at_rows], du_hbm.at[at_rows], out_sem.at[0, i]).start()
-        pltpu.make_async_copy(dg.at[at_rows], dg_hbm.at[at_rows], out_sem.at[1, i]).start()
 
     def gathered(j):
         @pl.when(j != k)
@@ -294,14 +292,6 @@
                 across(block, block, as_sem.at[j, c], ar_sem.at[j, c]).wait_send()
 
     loop(0, n, sent_across)
-
-    def stored(i):
-        at_rows = pl.ds(pl.multiple_of(i * brows, brows), brows)
-        pltpu.make_async_copy(du.at[at_rows], du_hbm.at[at_rows], out_sem.at[0, i]).wait()
-        pltpu.make_async_copy(dg.at[at_rows], dg_hbm.at[at_rows], out_sem.at[1, i]).wait()
-
-    loop(0, blocks, stored)
-    loop(0, PIECES, lambda p: pltpu.make_async_copy(gd.at[p], gd_hbm.at[p], gd_sem.at[p]).wait())
 
     for t in range(1, n):
         energy_copy(k, lax.rem(k + t, n)).wait_recv()
@@ -313,6 +303,18 @@
         energy_copy(lax.rem(k + t, n), k).wait_send()
 
 
+def write_out(dg, du, gd, en, dg_hbm, du_hbm, gd_hbm, en_out, sem):
+    copies = [
+        pltpu.make_async_copy(src, dst, sem.at[i])
+        for i, (src, dst) in enumerate(((dg, dg_hbm), (du, du_hbm), (gd, gd_hbm)))
+    ]
+    for copy in copies:
+        copy.start()
+    en_out[...] = en[0, :]
+    for copy in copies:
+        copy.wait()
+
+
 def fused(n, gate_pre, up_pre, out_grad, w_down):
     tokens, units = gate_pre.shape
     width = out_grad.shape[1]
@@ -321,24 +323,22 @@
     count = PIECES - SPLIT
     factor = float(tokens * lax.axis_size("rep") * n) ** (-0.5)
     any_spec = pl.BlockSpec(memory_space=pl.ANY)
+    vmem_spec = pl.BlockSpec(memory_space=pltpu.VMEM)
     dma = pltpu.SemaphoreType.DMA
     d_gate, d_up, grad, energy = pl.pallas_call(
         functools.partial(kernel, n, factor, width),
         out_shape=(
-            jax.ShapeDtypeStruct((tokens, units), BF16),
-            jax.ShapeDtypeStruct((tokens, units), BF16),
-            jax.ShapeDtypeStruct((PIECES, rows, cols), F32),
-            jax.ShapeDtypeStruct((1, units), F32),
+            pltpu.VMEM((tokens, units), BF16),
+            pltpu.VMEM((tokens, units), BF16),
+            pltpu.VMEM((PIECES, rows, cols), F32),
+            pltpu.VMEM((1, units), F32),
         ),
         in_specs=[any_spec] * 4,
-        out_specs=(any_spec, any_spec, any_spec, pl.BlockSpec(memory_space=pltpu.VMEM)),
+        out_specs=(vmem_spec,) * 4,
         scratch_shapes=[
             pltpu.VMEM((tokens, units), BF16),
             pltpu.VMEM((tokens, units), BF16),
             pltpu.VMEM((n, tokens, cols), BF16),
-            pltpu.VMEM((tokens, units), BF16),
-            pltpu.VMEM((tokens, units), BF16),
-            pltpu.VMEM((PIECES, rows, cols), F32),
             pltpu.VMEM((n, PIECES, rows, cols), BF16),
             pltpu.VMEM((units, tokens), BF16),
             pltpu.VMEM((n, PIECES, rows, cols), F32),
@@ -352,8 +352,6 @@
             pltpu.VMEM((8, units), F32),
             pltpu.VMEM((n, 8, units), F32),
             dma((3 + n,)),
-            dma((2, 4)),
-            dma((PIECES,)),
             dma((2, n, count)),
             dma((2, n, count)),
             dma((n, SPLIT)),
@@ -366,10 +364,22 @@
             dma((n,)),
         ],
         compiler_params=pltpu.CompilerParams(
-            collective_id=0, has_side_effects=True, vmem_limit_bytes=60 * 1024 * 1024
+            collective_id=0, has_side_effects=True, vmem_limit_bytes=VMEM_LIMIT
         ),
     )(gate_pre, up_pre, out_grad, w_down.reshape(PIECES, rows, cols))
-    return d_gate, d_up, grad.reshape(units, cols), energy.reshape(units)
+    return pl.pallas_call(
+        write_out,
+        out_shape=(
+            jax.ShapeDtypeStruct((tokens, units), BF16),
+            jax.ShapeDtypeStruct((tokens, units), BF16),
+            jax.ShapeDtypeStruct((units, cols), F32),
+            jax.ShapeDtypeStruct((units,), F32),
+        ),
+        in_specs=[vmem_spec] * 4,
+        out_specs=(any_spec, any_spec, any_spec, vmem_spec),
+        scratch_shapes=[dma((3,))],
+        compiler_params=pltpu.CompilerParams(vmem_limit_bytes=4 * 1024 * 1024),
+    )(d_gate, d_up, grad.reshape(units, cols), energy)
 
 
 def solution(mesh):

time: 75.3 us -> 68.8 us (0.914)
  local copies, waits for them, and re-layouts: 5.89 us -> 0 us
  other arithmetic: 1.28 us -> 0 us
    unnamed x7 -> x0, local copies, waits for them, and re-layouts: 5.89 us -> none
    pallas_call x1 -> x0, other arithmetic: 1.28 us -> none  [fused(): pl.pallas_call(functools.partial(kernel, n, factor, width), out_shape=(ja...]
    pallas_call x1 -> x2, Pallas kernels: 67.3 us -> 68 us  [the longest x1 65.3 us: fused(): pl.pallas_call(functools.partial(kernel, n, factor, width), out_shape=(pl...]
where the time goes in v2:
time: 68.8 us; the launch traced here: 68.7 us
  Pallas kernels  68 us (99%)
    pallas_call x1, Pallas kernels, fused(): pl.pallas_call(functools.partial(kernel, n, factor, width), out_shape=(pl...  65.3 us
    pallas_call x1, Pallas kernels, fused(): pl.pallas_call(write_out, out_shape=(jax.ShapeDtypeStruct((tokens, units)...  2.78 us

profile of v2, /device:TPU:0, one launch (start us, length us, event | category | flops | bytes accessed | tf_op | source)
XLA Modules:
  0.0 68.7 jit_solution(10482607929492747505)
XLA Ops:
  0.6 65.3 %shard_map.75 = (bf16[1024,768]{1,0:T(8,128)(2,1)S(1)}, bf16[1024,768]{1,0:T(8,128)(2,1)S(1)}, f32[6,128,512]{2,1,0:T(8,128)S(1)}, f32[1,768]{1,0:T(1,128)S(1)}) custom-call(bf16[1024,768]{1,0:T(8,128)(2,1)} %g_hbm.1, bf16[1024,768]{1,0:T(8,128)(2,1)} %u_hbm.1, bf16[1024,2048]{1,0:T(8,128)(2,1)} %og_hbm.1, bf16[6,128,512]{2,1,0:T(8,128)(2,1)} %bitcast.3), custom_call_target="tpu_custom_call" | custom-call | tf_op jit(solution)/shard_map/pallas_call | solution.py:328
  65.9 2.8 %shard_map.76 = (bf16[1024,768]{1,0:T(8,128)(2,1)}, bf16[1024,768]{1,0:T(8,128)(2,1)}, f32[768,512]{1,0:T(8,128)}, f32[768]{0:T(1024)}) custom-call(bf16[1024,768]{1,0:T(8,128)(2,1)S(1)} %get-tuple-element.8.dg, bf16[1024,768]{1,0:T(8,128)(2,1)S(1)} %get-tuple-element.9.du, f32[768,512]{1,0:T(8,128)S(1)} %bitcast.2, f32[1,768]{1,0:T(1,128)S(1)} %get-tuple-element.11.en), custom_call_target="tpu_custom_call" | custom-call | tf_op jit(solution)/shard_map/pallas_call | solution.py:370
